TPU v7x, 32 devices: a whole 2x2x4 slice. The times are simulated.
32 devices in a mesh: ep: 4 (over y, x), tp: 8 (over z, core).
Axes of the slice: x: 2, y: 2, z: 4, core: 2. Of those that a mesh axis runs over, the one named last changes fastest.
Arguments:
- tokens: bfloat16 [2048, 2048], P('ep', 'tp'), may hold values from -6 to 6
- norm_gain: float32 [2048], replicated, may hold values from 0.1 to 1.9
- norm_shift: float32 [2048], replicated, may hold values from -3 to 3
- expert_ids: int32 [2048, 6], P('ep'), may hold values from 0 to 31, all different within a row; in each aligned block of 64 rows (0 to 63, 64 to 127, ...) at most 24 rows name the same one
- affinity: float32 [2048, 6], P('ep'), may hold values from 0.05 to 1
- expert_gate: bfloat16 [32, 2048, 512], P(('ep', 'tp')), may hold values from -0.125 to 0.125
- expert_up: bfloat16 [32, 2048, 512], P(('ep', 'tp')), may hold values from -0.125 to 0.125
- expert_down: bfloat16 [32, 512, 2048], P(('ep', 'tp')), may hold values from -0.25 to 0.25
- shared_gate: bfloat16 [512, 2048], P('tp'), may hold values from -0.125 to 0.125
- shared_up: bfloat16 [512, 2048], P('tp'), may hold values from -0.125 to 0.125
- shared_down: bfloat16 [512, 2048], replicated, may hold values from -0.25 to 0.25
Outputs:
- mixed: bfloat16 [2048, 2048], P(('ep', 'tp'))
Inputs may be any that keep to these rules, and one draw needn't show every extreme that they name: `expert_ids`: each row names 6 different experts; in each aligned block of 64 rows (the rows of one device of tp) no expert is named more than 24 times, and in some blocks an expert is named exactly 24 times.
All inputs are finite; a program needn't handle non-finite values.
Results may differ from a plain program's by a relative error of at most 0.0069.
Values may be sent and summed in bfloat16 or wider, within the bound.
A program may use at most 64 MiB of HBM per device.

v0:
```python
import jax
import jax.numpy as jnp
from jax import lax
from jax.sharding import PartitionSpec as P

ROUTED_SCALE = 2.5
EPSILON = 1e-05


def pair_ranks(flat_ids, expert_count):
    onehot = flat_ids[..., None] == jnp.arange(expert_count, dtype=jnp.int32)
    running = jnp.cumsum(onehot.astype(jnp.int32), axis=-2)
    return jnp.sum(jnp.where(onehot, running, 0), axis=-1) - 1


def expert_rows(tok_rows, w_gate, w_up, w_down):
    gate_act = jnp.dot(tok_rows, w_gate, preferred_element_type=jnp.float32)
    up_act = jnp.dot(tok_rows, w_up, preferred_element_type=jnp.float32)
    hidden = (jax.nn.silu(gate_act) * up_act).astype(jnp.bfloat16)
    return jnp.dot(hidden, w_down, preferred_element_type=jnp.float32).astype(jnp.bfloat16)


def weighted_sum(source_rows, slot_index, pair_weight, top_count):
    total = jnp.zeros((slot_index.shape[0], source_rows.shape[1]), jnp.float32)
    for column in range(top_count):
        picked = jnp.take(source_rows, slot_index[:, column], axis=0, mode="fill", fill_value=0)
        total = total + pair_weight[:, column : column + 1] * picked.astype(jnp.float32)
    return total


def on_device(
    tokens,
    norm_gain,
    norm_shift,
    expert_ids,
    affinity,
    expert_gate,
    expert_up,
    expert_down,
    shared_gate,
    shared_up,
    shared_down,
):
    ep_count = lax.axis_size("ep")
    tp_count = lax.axis_size("tp")
    tp_index = lax.axis_index("tp")
    whole = lax.all_gather(tokens, "tp", axis=1, tiled=True)
    tok_count = whole.shape[0]
    width = whole.shape[1]
    top_count = expert_ids.shape[1]
    block_rows = tok_count // tp_count
    expert_count = ep_count * tp_count
    slot_cap = max(1, 2 * block_rows * top_count // expert_count)
    slot_total = expert_count * slot_cap
    values = whole.astype(jnp.float32)
    center = values - jnp.mean(values, axis=1, keepdims=True)
    spread = jnp.mean(center * center, axis=1, keepdims=True)
    normed = (center * lax.rsqrt(spread + EPSILON) * norm_gain + norm_shift).astype(jnp.bfloat16)
    weights = affinity / jnp.sum(affinity, axis=1, keepdims=True) * ROUTED_SCALE
    contract = (((1,), (1,)), ((), ()))
    shared_g = lax.dot_general(shared_gate, normed, contract, preferred_element_type=jnp.float32)
    shared_u = lax.dot_general(shared_up, normed, contract, preferred_element_type=jnp.float32)
    shared_hidden = (jax.nn.silu(shared_g) * shared_u).astype(jnp.bfloat16)
    own_hidden = lax.all_to_all(shared_hidden, "tp", split_axis=1, concat_axis=0, tiled=True)
    shared_out = lax.dot_general(
        own_hidden, shared_down, (((0,), (0,)), ((), ())), preferred_element_type=jnp.float32
    )
    block_ids = expert_ids.reshape(tp_count, block_rows * top_count)
    ranks = pair_ranks(block_ids, expert_count)
    group_index = block_ids // tp_count
    mine = block_ids % tp_count == tp_index
    block_index = jnp.arange(tp_count, dtype=jnp.int32)[:, None]
    dest = jnp.where(mine, (group_index * tp_count + block_index) * slot_cap + ranks, slot_total)
    token_index = (
        block_index * block_rows
        + jnp.arange(block_rows * top_count, dtype=jnp.int32)[None, :] // top_count
    )
    source_row = (
        jnp.full((slot_total + 1,), tok_count, jnp.int32)
        .at[dest.reshape(-1)]
        .set(token_index.reshape(-1))[:slot_total]
    )
    outgoing = jnp.take(normed, source_row, axis=0, mode="fill", fill_value=0).reshape(
        ep_count, tp_count, slot_cap, width
    )
    incoming = lax.all_to_all(outgoing, "ep", split_axis=0, concat_axis=0, tiled=True)
    result = expert_rows(incoming.reshape(-1, width), expert_gate[0], expert_up[0], expert_down[0])
    returned = lax.all_to_all(
        result.reshape(incoming.shape), "ep", split_axis=0, concat_axis=0, tiled=True
    )
    pair_slot = dest.reshape(tok_count, top_count)
    back_rows = returned.reshape(slot_total, width)
    routed = lax.psum_scatter(
        weighted_sum(back_rows, pair_slot, weights, top_count),
        "tp",
        scatter_dimension=0,
        tiled=True,
    )
    return (routed + shared_out).astype(jnp.bfloat16)


def solution(mesh):
    placed = (
        P("ep", "tp"),
        P(),
        P(),
        P("ep", None),
        P("ep", None),
        P(("ep", "tp"), None, None),
        P(("ep", "tp"), None, None),
        P(("ep", "tp"), None, None),
        P("tp", None),
        P("tp", None),
        P(),
    )
    return jax.shard_map(
        on_device, mesh=mesh, in_specs=placed, out_specs=P(("ep", "tp"), None), check_vma=False
    )
```

profile of v0, /device:TPU:0, one launch (start us, length us, event | category | flops | bytes accessed | tf_op | source)
XLA Modules:
  0.0 271.8 jit_solution(16597467197731617035)
XLA Ops:
  8.8 6.9 %reduce-window.6 = s32[8,32,3,128]{3,1,2,0:T(8,128)S(1)} reduce-window(s32[8,32,3,128]{3,1,2,0:T(8,128)S(1)} %fusion.20, s32[]{:T(128)} %constant.82.clone.1), window={size=1x1x1x128 pad=0_0x0_0x0_0x127_0}, to_apply=%region_1.0 | reduce-window | flops 12484608 | bytes 786436 | tf_op jit(solution)/shard_map/reduce-window
  16.6 11.8 %scatter_custom_fusion = s32[769]{0:T(1024)S(1)} fusion(s32[3072]{0:T(1024)S(1)} %bitcast.82, s32[3072]{0:T(1024)S(1)} %reshape.307, s32[]{:T(128)} %constant.81.clone.1), kind=kCustom, calls=%fused_computation.94 | custom fusion | bytes 3080 | tf_op jit(solution)/shard_map/scatter | solution.py:81
  28.5 13.8 %all-gather.2.cloned.1.call-done = bf16[512,2048]{1,0:T(8,128)(2,1)} async-done(((bf16[512,256]{1,0:T(8,128)(2,1)}), bf16[512,2048]{1,0:T(8,128)(2,1)}) %all-gather.2.cloned.1.call-update) | async-done | bytes 2097168 | tf_op jit(solution)/shard_map/all_gather | solution.py:47
  42.3 2.1 convert_reduce_fusion
  45.2 2.2 fusion.5
  47.4 9.0 %gather_fusion = bf16[768,2048]{1,0:T(8,128)(2,1)} fusion(bf16[512,2048]{1,0:T(8,128)(2,1)} %fusion.5, s32[1024]{0:T(1024)S(1)} %pad_clamp_fusion.6), kind=kCustom, calls=%fused_computation.6 | custom fusion | bytes 6294528 | tf_op jit(solution)/shard_map/jit(_take)/gather | solution.py:83
  56.4 3.9 %broadcast_select_fusion = bf16[4,8,24,2048]{3,2,1,0:T(8,128)(2,1)} fusion(bf16[4,8,24,2048]{3,2,1,0:T(8,128)(2,1)} %bitcast.77, pred[4,8,24]{2,1,0:T(8,128)(4,1)S(1)} %compare_and_fusion), kind=kLoop, calls=%fused_computation.18 | loop fusion | flops 1572864 | bytes 6292224 | tf_op jit(solution)/shard_map/jit(_take)/select_n | solution.py:83
  60.3 4.9 %all-to-all-start = ((bf16[4,8,24,2048]{3,2,1,0:T(8,128)(2,1)}), bf16[4,8,24,2048]{3,2,1,0:T(8,128)(2,1)}, u32[]{:S(2)}, u32[]{:S(2)}) async-start(bf16[4,8,24,2048]{3,2,1,0:T(8,128)(2,1)} %broadcast_select_fusion), calls=%async_computation | async-start | bytes 6291456 | tf_op jit(solution)/shard_map/all_to_all | solution.py:86
  66.7 35.2 %all-to-all-done = bf16[4,8,24,2048]{3,2,1,0:T(8,128)(2,1)} async-done(((bf16[4,8,24,2048]{3,2,1,0:T(8,128)(2,1)}), bf16[4,8,24,2048]{3,2,1,0:T(8,128)(2,1)}, u32[]{:S(2)}, u32[]{:S(2)}) %all-to-all-start) | async-done | bytes 3145760 | tf_op jit(solution)/shard_map/all_to_all | solution.py:86
  101.9 5.6 %fusion.10 = f32[768,512]{1,0:T(8,128)} fusion(bf16[768,2048]{1,0:T(8,128)(2,1)} %bitcast.5, bf16[1,2048,512]{2,1,0:T(8,128)(2,1)} %param.18), kind=kOutput, calls=%fused_computation.24 | convolution fusion | flops 1610612736 | bytes 6815744 | tf_op jit(solution)/shard_map/dot_general | solution.py:17
  107.4 8.2 %convolution_convert_fusion = bf16[768,2048]{1,0:T(8,128)(2,1)} fusion(bf16[1,512,2048]{2,1,0:T(8,128)(2,1)S(1)} %copy-done, f32[768,512]{1,0:T(8,128)} %fusion.10, bf16[768,2048]{1,0:T(8,128)(2,1)} %bitcast.5, bf16[1,2048,512]{2,1,0:T(8,128)(2,1)} %param.19), kind=kOutput, calls=%fused_computation.17 | convolution fusion | flops 3225157632 | bytes 12058624 | tf_op jit(solution)/shard_map/dot_general | solution.py:20
  115.6 4.6 %all-to-all-start.1 = ((bf16[4,8,24,2048]{3,2,1,0:T(8,128)(2,1)}), bf16[4,8,24,2048]{3,2,1,0:T(8,128)(2,1)}, u32[]{:S(2)}, u32[]{:S(2)}) async-start(bf16[4,8,24,2048]{3,2,1,0:T(8,128)(2,1)} %bitcast.78), calls=%async_computation.1 | async-start | bytes 6291456 | tf_op jit(solution)/shard_map/all_to_all | solution.py:88
  120.5 35.7 %all-to-all-done.1 = bf16[4,8,24,2048]{3,2,1,0:T(8,128)(2,1)} async-done(((bf16[4,8,24,2048]{3,2,1,0:T(8,128)(2,1)}), bf16[4,8,24,2048]{3,2,1,0:T(8,128)(2,1)}, u32[]{:S(2)}, u32[]{:S(2)}) %all-to-all-start.1) | async-done | bytes 3145760 | tf_op jit(solution)/shard_map/all_to_all | solution.py:88
  156.2 7.8 %gather_fusion.6 = bf16[512,2048]{1,0:T(8,128)(2,1)} fusion(bf16[768,2048]{1,0:T(8,128)(2,1)} %bitcast.10, s32[1024]{0:T(1024)S(1)} %pad_clamp_fusion), kind=kCustom, calls=%fused_computation.5.clone | custom fusion | bytes 4196352 | tf_op jit(solution)/shard_map/jit(_take)/gather | solution.py:26
  164.0 7.5 %gather_fusion.5 = bf16[512,2048]{1,0:T(8,128)(2,1)} fusion(bf16[768,2048]{1,0:T(8,128)(2,1)} %bitcast.10, s32[1024]{0:T(1024)S(1)} %pad_clamp_fusion.1), kind=kCustom, calls=%fused_computation.4.clone | custom fusion | bytes 4196352 | tf_op jit(solution)/shard_map/jit(_take)/gather | solution.py:26
  171.6 7.5 %gather_fusion.4 = bf16[512,2048]{1,0:T(8,128)(2,1)} fusion(bf16[768,2048]{1,0:T(8,128)(2,1)} %bitcast.10, s32[1024]{0:T(1024)S(1)} %pad_clamp_fusion.2), kind=kCustom, calls=%fused_computation.3.clone | custom fusion | bytes 4196352 | tf_op jit(solution)/shard_map/jit(_take)/gather | solution.py:26
  179.1 7.5 %gather_fusion.3 = bf16[512,2048]{1,0:T(8,128)(2,1)} fusion(bf16[768,2048]{1,0:T(8,128)(2,1)} %bitcast.10, s32[1024]{0:T(1024)S(1)} %pad_clamp_fusion.3), kind=kCustom, calls=%fused_computation.2.clone | custom fusion | bytes 4196352 | tf_op jit(solution)/shard_map/jit(_take)/gather | solution.py:26
  186.6 7.5 %gather_fusion.2 = bf16[512,2048]{1,0:T(8,128)(2,1)} fusion(bf16[768,2048]{1,0:T(8,128)(2,1)} %bitcast.10, s32[1024]{0:T(1024)S(1)} %pad_clamp_fusion.4), kind=kCustom, calls=%fused_computation.1.clone | custom fusion | bytes 4196352 | tf_op jit(solution)/shard_map/jit(_take)/gather | solution.py:26
  194.1 7.8 %gather_fusion.1 = bf16[512,2048]{1,0:T(8,128)(2,1)} fusion(bf16[768,2048]{1,0:T(8,128)(2,1)} %bitcast.10, s32[1024]{0:T(1024)S(1)} %pad_clamp_fusion.5), kind=kCustom, calls=%fused_computation.clone | custom fusion | bytes 4196352 | tf_op jit(solution)/shard_map/jit(_take)/gather | solution.py:26
  202.0 9.0 %multiply_add_fusion = f32[512,2048]{1,0:T(8,128)} fusion(bf16[512,2048]{1,0:T(8,128)(2,1)} %gather_fusion.6, bf16[512,2048]{1,0:T(8,128)(2,1)} %gather_fusion.5, bf16[512,2048]{1,0:T(8,128)(2,1)} %gather_fusion.4, bf16[512,2048]{1,0:T(8,128)(2,1)} %gather_fusion.3, bf16[512,2048]{1,0:T(8,128)(2,1)} %gather_fusion.2, bf16[512,2048]{1,0:T(8,128)(2,1)} %gather_fusion.1, ...), kind=kLoop, calls=%fused_computation.16 | loop fusion | flops 24117248 | bytes 16792576 | tf_op jit(solution)/shard_map/add | solution.py:27
  212.0 2.5 convolution_bitcast_fusion.1
  215.6 11.3 %all_to_all.29 = bf16[8,2,2048]{2,1,0:T(2,128)(2,1)S(1)} all-to-all(bf16[8,2,2048]{2,1,0:T(2,128)(2,1)S(1)} %reshape.338), channel_id=1, replica_groups=mesh['ep'=4,'tp'=8] {'tp'}, dimensions={0} | all-to-all | bytes 131072 | tf_op jit(solution)/shard_map/all_to_all | solution.py:64
  227.3 34.9 %reduce-scatter.2.cloned.1.call-done = f32[64,2048]{1,0:T(8,128)} async-done(((f32[512,2048]{1,0:T(8,128)}), f32[64,2048]{1,0:T(8,128)}) %reduce-scatter.2.cloned.1.call-update) | async-done | bytes 524304 | tf_op jit(solution)/shard_map/reduce_scatter | solution.py:93
  262.1 2.9 %fusion.6 = bf16[64,2048]{1,0:T(8,128)(2,1)} fusion(f32[64,2048]{1,0:T(8,128)} %reduce-scatter.2.cloned.1.call-done, bf16[512,64]{0,1:T(8,128)(2,1)S(1)} %all_to_all.25, bf16[512,2048]{1,0:T(8,128)(2,1)} %param.23), kind=kOutput, calls=%fused_computation.20 | convolution fusion | flops 134479872 | bytes 2949120 | tf_op jit(solution)/shard_map/dot_general | solution.py:65
  (74 shorter events, 7.9 us)
Async XLA Ops:
  6.5 100.9 %copy-start = (bf16[1,512,2048]{2,1,0:T(8,128)(2,1)S(1)}, bf16[1,512,2048]{2,1,0:T(8,128)(2,1)}, u32[]{:S(2)}) copy-start(bf16[1,512,2048]{2,1,0:T(8,128)(2,1)} %param.20) | copy-start | bytes 6291460
  6.5 35.8 %all-gather.2.cloned.1.call-start = ((), (), s32[]{:S(2)}) async-start(), calls=%async_computation.4 | async-start | bytes 2359296 | tf_op jit(solution)/shard_map/all_gather | solution.py:47
  42.3 2.2 copy-start.2
  42.3 2.9 %copy-start.5 = (f32[2048]{0:T(1024)S(1)}, f32[2048]{0:T(1024)}, u32[]{:S(2)}) copy-start(f32[2048]{0:T(1024)} %param.15) | copy-start | bytes 24580
  42.3 2.9 %copy-start.6 = (f32[2048]{0:T(1024)S(1)}, f32[2048]{0:T(1024)}, u32[]{:S(2)}) copy-start(f32[2048]{0:T(1024)} %param.14) | copy-start | bytes 24580
  60.3 5.3 %copy-start.4 = (f32[512,6]{0,1:T(8,128)S(1)}, f32[512,6]{0,1:T(8,128)}, u32[]{:S(2)}) copy-start(f32[512,6]{0,1:T(8,128)} %param.17) | copy-start | bytes 36868
  60.3 41.6 %all-to-all-start = ((bf16[4,8,24,2048]{3,2,1,0:T(8,128)(2,1)}), bf16[4,8,24,2048]{3,2,1,0:T(8,128)(2,1)}, u32[]{:S(2)}, u32[]{:S(2)}) async-start(bf16[4,8,24,2048]{3,2,1,0:T(8,128)(2,1)} %broadcast_select_fusion), calls=%async_computation | async-start | bytes 6291456 | tf_op jit(solution)/shard_map/all_to_all | solution.py:86
  115.6 40.6 %all-to-all-start.1 = ((bf16[4,8,24,2048]{3,2,1,0:T(8,128)(2,1)}), bf16[4,8,24,2048]{3,2,1,0:T(8,128)(2,1)}, u32[]{:S(2)}, u32[]{:S(2)}) async-start(bf16[4,8,24,2048]{3,2,1,0:T(8,128)(2,1)} %bitcast.78), calls=%async_computation.1 | async-start | bytes 6291456 | tf_op jit(solution)/shard_map/all_to_all | solution.py:88
  120.3 141.9 %reduce-scatter.2.cloned.1.call-start = ((), (), s32[]{:S(2)}) async-start(), calls=%async_computation.5 | async-start | bytes 4718592 | tf_op jit(solution)/shard_map/reduce_scatter | solution.py:93
  211.0 0.9 copy-start.3
  212.0 2.5 copy-start.1
  212.0 2.5 copy-start.7
Sparse Core Ops, SparseCore 0:
  8.9 33.3 all-gather.1
  211.2 50.8 reduce-scatter.1
where the time goes:
time: 273 us; the launch traced here: 272 us
  waiting for transfers between devices  120 us (44%)
  local copies, waits for them, and re-layouts  71.2 us (26%)
  other arithmetic  25.8 us (9%)
  matrix products  19.9 us (7%)
  between operations  13.8 us (5%)
  blocking collectives  11.3 us (4%)
  starting transfers between devices  9.63 us (4%)
    gather x6, local copies, waits for them, and re-layouts, weighted_sum(): jnp.take(source_rows, slot_index[:, column], axis=0, mode='fill', fill_va...  45.7 us
    all_to_all x1, waiting for transfers between devices, on_device(): lax.all_to_all(result.reshape(incoming.shape), 'ep', split_axis=0, concat...  35.7 us
    all_to_all x1, waiting for transfers between devices, on_device(): lax.all_to_all(outgoing, 'ep', split_axis=0, concat_axis=0, tiled=True)  35.2 us
    reduce_scatter x1, waiting for transfers between devices, on_device(): lax.psum_scatter(weighted_sum(back_rows, pair_slot, weights, top_count),...  34.9 us
    all_gather x1, waiting for transfers between devices, on_device(): whole = lax.all_gather(tokens, 'tp', axis=1, tiled=True)  13.8 us
    scatter x1, local copies, waits for them, and re-layouts, on_device(): source_row = jnp.full((slot_total + 1,), tok_count, jnp.int32).at[dest.re...  11.8 us
    all_to_all x1, blocking collectives, on_device(): lax.all_to_all(shared_hidden, 'tp', split_axis=1, concat_axis=0, tiled=True)  11.3 us
    add x1, other arithmetic, weighted_sum(): total + pair_weight[:, column:column + 1] * picked.astype(jnp.float32)  9.05 us
  transfers between devices with their start and end apart: 4, of which 4 were waited for; matrix products, arithmetic and copies ran while one was open for 10% of the time, Pallas kernels for 0%

commit v1 on v0

--- a/solution.py
+++ b/solution.py
@@ -44,7 +44,12 @@
     ep_count = lax.axis_size("ep")
     tp_count = lax.axis_size("tp")
     tp_index = lax.axis_index("tp")
-    whole = lax.all_gather(tokens, "tp", axis=1, tiled=True)
+    ring = [tokens]
+    for hop in range(7):
+        ring.append(lax.ppermute(ring[-1], "tp", [(dev, (dev + 1) % 8) for dev in range(8)]))
+    whole = jnp.roll(
+        jnp.concatenate(ring[::-1], axis=1), (lax.axis_index("tp") + 1) * ring[0].shape[1], axis=1
+    )
     tok_count = whole.shape[0]
     width = whole.shape[1]
     top_count = expert_ids.shape[1]

time: 273 us -> 302 us (1.11)
  waiting for transfers between devices: 120 us -> 136 us
  local copies, waits for them, and re-layouts: 71.2 us -> 81 us
    ppermute x0 -> x7, waiting for transfers between devices: none -> 38.2 us  [on_device(): lax.ppermute(ring[-1], 'tp', [(dev, (dev + 1) % 8) for dev in range(8)])]
    all_gather x1 -> x0, waiting for transfers between devices: 13.8 us -> none  [on_device(): whole = lax.all_gather(tokens, 'tp', axis=1, tiled=True)]
    unnamed x22 -> x35, local copies, waits for them, and re-layouts: 2.26 us -> 12 us
    all_to_all x1, waiting for transfers between devices: 35.2 us -> 29.4 us  [on_device(): lax.all_to_all(outgoing, 'ep', split_axis=0, concat_axis=0, tiled=True)]
  transfers between devices with their start and end apart: 4 -> 10, of which waited for: 4 -> 8; matrix products, arithmetic and copies ran while one was open for 10% -> 9% of each run, Pallas kernels for 0% -> 0%
where the time goes in v1:
time: 302 us; the launch traced here: 301 us
  waiting for transfers between devices  136 us (45%)
  local copies, waits for them, and re-layouts  81 us (27%)
  other arithmetic  24 us (8%)
  matrix products  21.3 us (7%)
  between operations  14 us (5%)
  blocking collectives  13.2 us (4%)
  starting transfers between devices  10.6 us (4%)
    gather x6, local copies, waits for them, and re-layouts, weighted_sum(): jnp.take(source_rows, slot_index[:, column], axis=0, mode='fill', fill_va...  45.7 us
    ppermute x7, waiting for transfers between devices, on_device(): lax.ppermute(ring[-1], 'tp', [(dev, (dev + 1) % 8) for dev in range(8)])  38.2 us
    all_to_all x1, waiting for transfers between devices, on_device(): lax.all_to_all(result.reshape(incoming.shape), 'ep', split_axis=0, concat...  35.4 us
    reduce_scatter x1, waiting for transfers between devices, on_device(): lax.psum_scatter(weighted_sum(back_rows, pair_slot, weights, top_count),...  33.4 us
    all_to_all x1, waiting for transfers between devices, on_device(): lax.all_to_all(outgoing, 'ep', split_axis=0, concat_axis=0, tiled=True)  29.4 us
    all_to_all x1, blocking collectives, on_device(): lax.all_to_all(shared_hidden, 'tp', split_axis=1, concat_axis=0, tiled=True)  13.2 us
    unnamed x35, local copies, waits for them, and re-layouts  12 us
    scatter x1, local copies, waits for them, and re-layouts, on_device(): source_row = jnp.full((slot_total + 1,), tok_count, jnp.int32).at[dest.re...  11.8 us
  transfers between devices with their start and end apart: 10, of which 8 were waited for; matrix products, arithmetic and copies ran while one was open for 9% of the time, Pallas kernels for 0%

profile of v1, /device:TPU:0, one launch (start us, length us, event | category | flops | bytes accessed | tf_op | source)
XLA Modules:
  0.0 300.7 jit_solution(13491638563608755057)
XLA Ops:
  7.0 8.4 %collective-permute-done = bf16[512,256]{1,0:T(8,128)(2,1)} collective-permute-done((bf16[512,256]{1,0:T(8,128)(2,1)}, bf16[512,256]{1,0:T(8,128)(2,1)}, u32[]{:S(2)}, u32[]{:S(2)}) %collective-permute-start) | collective-permute-done | bytes 262176 | tf_op jit(solution)/shard_map/ppermute | solution.py:49
  16.7 6.9 %reduce-window.6 = s32[8,32,3,128]{3,1,2,0:T(8,128)S(1)} reduce-window(s32[8,32,3,128]{3,1,2,0:T(8,128)S(1)} %fusion.20, s32[]{:T(128)} %constant.102.clone.1), window={size=1x1x1x128 pad=0_0x0_0x0_0x127_0}, to_apply=%region_1.2 | reduce-window | flops 12484608 | bytes 786436 | tf_op jit(solution)/shard_map/reduce-window
  24.7 7.1 %collective-permute-done.2 = bf16[512,256]{1,0:T(8,128)(2,1)S(1)} collective-permute-done((bf16[512,256]{1,0:T(8,128)(2,1)}, bf16[512,256]{1,0:T(8,128)(2,1)S(1)}, u32[]{:S(2)}, u32[]{:S(2)}) %collective-permute-start.2) | collective-permute-done | bytes 262176 | tf_op jit(solution)/shard_map/ppermute | solution.py:49
  32.1 7.3 %collective-permute-done.3 = bf16[512,256]{1,0:T(8,128)(2,1)S(1)} collective-permute-done((bf16[512,256]{1,0:T(8,128)(2,1)S(1)}, bf16[512,256]{1,0:T(8,128)(2,1)S(1)}, u32[]{:S(2)}, u32[]{:S(2)}) %collective-permute-start.3) | collective-permute-done | bytes 262176 | tf_op jit(solution)/shard_map/ppermute | solution.py:49
  39.6 7.6 %collective-permute-done.4 = bf16[512,256]{1,0:T(8,128)(2,1)} collective-permute-done((bf16[512,256]{1,0:T(8,128)(2,1)S(1)}, bf16[512,256]{1,0:T(8,128)(2,1)}, u32[]{:S(2)}, u32[]{:S(2)}) %collective-permute-start.4) | collective-permute-done | bytes 262176 | tf_op jit(solution)/shard_map/ppermute | solution.py:49
  47.2 11.8 %scatter_custom_fusion = s32[769]{0:T(1024)S(1)} fusion(s32[3072]{0:T(1024)S(1)} %bitcast.82, s32[3072]{0:T(1024)S(1)} %reshape.307, s32[]{:T(128)} %constant.101.clone.1), kind=kCustom, calls=%fused_computation.110 | custom fusion | bytes 3080 | tf_op jit(solution)/shard_map/scatter | solution.py:86
  59.2 7.8 %collective-permute-done.6 = bf16[512,256]{1,0:T(8,128)(2,1)} collective-permute-done((bf16[512,256]{1,0:T(8,128)(2,1)}, bf16[512,256]{1,0:T(8,128)(2,1)}, u32[]{:S(2)}, u32[]{:S(2)}) %collective-permute-start.6) | collective-permute-done | bytes 262176 | tf_op jit(solution)/shard_map/ppermute | solution.py:49
  80.4 9.0 %gather_fusion = bf16[768,2048]{1,0:T(8,128)(2,1)} fusion(bf16[512,2048]{1,0:T(8,128)(2,1)} %fusion.5, s32[1024]{0:T(1024)S(1)} %pad_clamp_fusion.6), kind=kCustom, calls=%fused_computation.6 | custom fusion | bytes 6294528 | tf_op jit(solution)/shard_map/jit(_take)/gather | solution.py:88
  89.3 3.9 %broadcast_select_fusion = bf16[4,8,24,2048]{3,2,1,0:T(8,128)(2,1)} fusion(bf16[4,8,24,2048]{3,2,1,0:T(8,128)(2,1)} %bitcast.77, pred[4,8,24]{2,1,0:T(8,128)(4,1)S(1)} %compare_and_fusion), kind=kLoop, calls=%fused_computation.18 | loop fusion | flops 1572864 | bytes 6292224 | tf_op jit(solution)/shard_map/jit(_take)/select_n | solution.py:88
  93.2 4.8 %all-to-all-start = ((bf16[4,8,24,2048]{3,2,1,0:T(8,128)(2,1)}), bf16[4,8,24,2048]{3,2,1,0:T(8,128)(2,1)}, u32[]{:S(2)}, u32[]{:S(2)}) async-start(bf16[4,8,24,2048]{3,2,1,0:T(8,128)(2,1)} %broadcast_select_fusion), calls=%async_computation | async-start | bytes 6291456 | tf_op jit(solution)/shard_map/all_to_all | solution.py:91
  99.5 29.4 %all-to-all-done = bf16[4,8,24,2048]{3,2,1,0:T(8,128)(2,1)} async-done(((bf16[4,8,24,2048]{3,2,1,0:T(8,128)(2,1)}), bf16[4,8,24,2048]{3,2,1,0:T(8,128)(2,1)}, u32[]{:S(2)}, u32[]{:S(2)}) %all-to-all-start) | async-done | bytes 3145760 | tf_op jit(solution)/shard_map/all_to_all | solution.py:91
  128.9 5.6 %fusion.10 = f32[768,512]{1,0:T(8,128)} fusion(bf16[768,2048]{1,0:T(8,128)(2,1)} %bitcast.5, bf16[1,2048,512]{2,1,0:T(8,128)(2,1)} %param.18), kind=kOutput, calls=%fused_computation.24 | convolution fusion | flops 1610612736 | bytes 6815744 | tf_op jit(solution)/shard_map/dot_general | solution.py:17
  134.5 8.2 %convolution_convert_fusion = bf16[768,2048]{1,0:T(8,128)(2,1)} fusion(bf16[1,512,2048]{2,1,0:T(8,128)(2,1)S(1)} %copy-done, f32[768,512]{1,0:T(8,128)} %fusion.10, bf16[768,2048]{1,0:T(8,128)(2,1)} %bitcast.5, bf16[1,2048,512]{2,1,0:T(8,128)(2,1)} %param.19), kind=kOutput, calls=%fused_computation.17 | convolution fusion | flops 3225157632 | bytes 12058624 | tf_op jit(solution)/shard_map/dot_general | solution.py:20
  142.6 4.8 %all-to-all-start.1 = ((bf16[4,8,24,2048]{3,2,1,0:T(8,128)(2,1)}), bf16[4,8,24,2048]{3,2,1,0:T(8,128)(2,1)}, u32[]{:S(2)}, u32[]{:S(2)}) async-start(bf16[4,8,24,2048]{3,2,1,0:T(8,128)(2,1)} %bitcast.78), calls=%async_computation.1 | async-start | bytes 6291456 | tf_op jit(solution)/shard_map/all_to_all | solution.py:93
  147.7 35.4 %all-to-all-done.1 = bf16[4,8,24,2048]{3,2,1,0:T(8,128)(2,1)} async-done(((bf16[4,8,24,2048]{3,2,1,0:T(8,128)(2,1)}), bf16[4,8,24,2048]{3,2,1,0:T(8,128)(2,1)}, u32[]{:S(2)}, u32[]{:S(2)}) %all-to-all-start.1) | async-done | bytes 3145760 | tf_op jit(solution)/shard_map/all_to_all | solution.py:93
  183.1 7.8 %gather_fusion.6 = bf16[512,2048]{1,0:T(8,128)(2,1)} fusion(bf16[768,2048]{1,0:T(8,128)(2,1)} %bitcast.10, s32[1024]{0:T(1024)S(1)} %get-tuple-element.22), kind=kCustom, calls=%fused_computation.5.clone | custom fusion | bytes 4196352 | tf_op jit(solution)/shard_map/jit(_take)/gather | solution.py:26
  190.9 7.5 %gather_fusion.5 = bf16[512,2048]{1,0:T(8,128)(2,1)} fusion(bf16[768,2048]{1,0:T(8,128)(2,1)} %bitcast.10, s32[1024]{0:T(1024)S(1)} %get-tuple-element.23), kind=kCustom, calls=%fused_computation.4.clone | custom fusion | bytes 4196352 | tf_op jit(solution)/shard_map/jit(_take)/gather | solution.py:26
  198.4 7.5 %gather_fusion.4 = bf16[512,2048]{1,0:T(8,128)(2,1)} fusion(bf16[768,2048]{1,0:T(8,128)(2,1)} %bitcast.10, s32[1024]{0:T(1024)S(1)} %get-tuple-element.24), kind=kCustom, calls=%fused_computation.3.clone | custom fusion | bytes 4196352 | tf_op jit(solution)/shard_map/jit(_take)/gather | solution.py:26
  206.0 7.5 %gather_fusion.3 = bf16[512,2048]{1,0:T(8,128)(2,1)} fusion(bf16[768,2048]{1,0:T(8,128)(2,1)} %bitcast.10, s32[1024]{0:T(1024)S(1)} %get-tuple-element.25), kind=kCustom, calls=%fused_computation.2.clone | custom fusion | bytes 4196352 | tf_op jit(solution)/shard_map/jit(_take)/gather | solution.py:26
  213.5 7.5 %gather_fusion.2 = bf16[512,2048]{1,0:T(8,128)(2,1)} fusion(bf16[768,2048]{1,0:T(8,128)(2,1)} %bitcast.10, s32[1024]{0:T(1024)S(1)} %get-tuple-element.26), kind=kCustom, calls=%fused_computation.1.clone | custom fusion | bytes 4196352 | tf_op jit(solution)/shard_map/jit(_take)/gather | solution.py:26
  221.0 7.8 %gather_fusion.1 = bf16[512,2048]{1,0:T(8,128)(2,1)} fusion(bf16[768,2048]{1,0:T(8,128)(2,1)} %bitcast.10, s32[1024]{0:T(1024)S(1)} %get-tuple-element.27), kind=kCustom, calls=%fused_computation.clone | custom fusion | bytes 4196352 | tf_op jit(solution)/shard_map/jit(_take)/gather | solution.py:26
  228.9 9.1 %multiply_add_fusion = f32[512,2048]{1,0:T(8,128)} fusion(bf16[512,2048]{1,0:T(8,128)(2,1)} %gather_fusion.6, bf16[512,2048]{1,0:T(8,128)(2,1)} %gather_fusion.5, bf16[512,2048]{1,0:T(8,128)(2,1)} %gather_fusion.4, bf16[512,2048]{1,0:T(8,128)(2,1)} %gather_fusion.3, bf16[512,2048]{1,0:T(8,128)(2,1)} %gather_fusion.2, bf16[512,2048]{1,0:T(8,128)(2,1)} %gather_fusion.1, ...), kind=kLoop, calls=%fused_computation.16 | loop fusion | flops 24117248 | bytes 16792576 | tf_op jit(solution)/shard_map/add | solution.py:27
  243.9 13.2 %all_to_all.29 = bf16[8,2,2048]{2,1,0:T(2,128)(2,1)S(1)} all-to-all(bf16[8,2,2048]{2,1,0:T(2,128)(2,1)S(1)} %reshape.338), channel_id=1, replica_groups=mesh['ep'=4,'tp'=8] {'tp'}, dimensions={0} | all-to-all | bytes 131072 | tf_op jit(solution)/shard_map/all_to_all | solution.py:69
  257.5 33.4 %reduce-scatter.2.cloned.1.call-done = f32[64,2048]{1,0:T(8,128)} async-done(((f32[512,2048]{1,0:T(8,128)}), f32[64,2048]{1,0:T(8,128)}) %reduce-scatter.2.cloned.1.call-update) | async-done | bytes 524304 | tf_op jit(solution)/shard_map/reduce_scatter | solution.py:98
  (99 shorter events, 27.3 us)
Async XLA Ops:
  6.5 127.9 %copy-start = (bf16[1,512,2048]{2,1,0:T(8,128)(2,1)S(1)}, bf16[1,512,2048]{2,1,0:T(8,128)(2,1)}, u32[]{:S(2)}) copy-start(bf16[1,512,2048]{2,1,0:T(8,128)(2,1)} %param.20) | copy-start | bytes 6291460
  6.5 8.9 %collective-permute-start = (bf16[512,256]{1,0:T(8,128)(2,1)}, bf16[512,256]{1,0:T(8,128)(2,1)}, u32[]{:S(2)}, u32[]{:S(2)}) collective-permute-start(bf16[512,256]{1,0:T(8,128)(2,1)} %param.13), channel_id=1, source_target_pairs={{0,1},{1,2},{2,3},{3,4},{4,5},{5,6},{6,7},{7,0},{8,9},{9,10},{10,1... | collective-permute-start | bytes 786440 | tf_op jit(solution)/shard_map/ppermute | solution.py:49
  15.4 8.6 %collective-permute-start.1 = (bf16[512,256]{1,0:T(8,128)(2,1)}, bf16[512,256]{1,0:T(8,128)(2,1)}, u32[]{:S(2)}, u32[]{:S(2)}) collective-permute-start(bf16[512,256]{1,0:T(8,128)(2,1)} %collective-permute-done), channel_id=1, source_target_pairs={{0,1},{1,2},{2,3},{3,4},{4,5},{5,6},{6,7},{7,0},{8,9},{9,10},{10,1... | collective-permute-start | bytes 786440 | tf_op jit(solution)/shard_map/ppermute | solution.py:49
  23.6 48.4 %copy-start.1 = (bf16[512,256]{1,0:T(8,128)(2,1)S(1)}, bf16[512,256]{1,0:T(8,128)(2,1)}, u32[]{:S(2)}) copy-start(bf16[512,256]{1,0:T(8,128)(2,1)} %param.13) | copy-start | bytes 786436
  24.0 7.9 %collective-permute-start.2 = (bf16[512,256]{1,0:T(8,128)(2,1)}, bf16[512,256]{1,0:T(8,128)(2,1)S(1)}, u32[]{:S(2)}, u32[]{:S(2)}) collective-permute-start(bf16[512,256]{1,0:T(8,128)(2,1)} %collective-permute-done.1), channel_id=1, source_target_pairs={{0,1},{1,2},{2,3},{3,4},{4,5},{5,6},{6,7},{7,0},{8,9},{9,10},{10,1... | collective-permute-start | bytes 786440 | tf_op jit(solution)/shard_map/ppermute | solution.py:49
  31.9 7.6 %collective-permute-start.3 = (bf16[512,256]{1,0:T(8,128)(2,1)S(1)}, bf16[512,256]{1,0:T(8,128)(2,1)S(1)}, u32[]{:S(2)}, u32[]{:S(2)}) collective-permute-start(bf16[512,256]{1,0:T(8,128)(2,1)S(1)} %collective-permute-done.2), channel_id=1, source_target_pairs={{0,1},{1,2},{2,3},{3,4},{4,5},{5,6},{6,7},{7,0},{8,9},{9,10},{10,1... | collective-permute-start | bytes 786440 | tf_op jit(solution)/shard_map/ppermute | solution.py:49
  39.5 7.7 %collective-permute-start.4 = (bf16[512,256]{1,0:T(8,128)(2,1)S(1)}, bf16[512,256]{1,0:T(8,128)(2,1)}, u32[]{:S(2)}, u32[]{:S(2)}) collective-permute-start(bf16[512,256]{1,0:T(8,128)(2,1)S(1)} %collective-permute-done.3), channel_id=1, source_target_pairs={{0,1},{1,2},{2,3},{3,4},{4,5},{5,6},{6,7},{7,0},{8,9},{9,10},{10,1... | collective-permute-start | bytes 786440 | tf_op jit(solution)/shard_map/ppermute | solution.py:49
  47.2 11.9 %collective-permute-start.5 = (bf16[512,256]{1,0:T(8,128)(2,1)}, bf16[512,256]{1,0:T(8,128)(2,1)}, u32[]{:S(2)}, u32[]{:S(2)}) collective-permute-start(bf16[512,256]{1,0:T(8,128)(2,1)} %collective-permute-done.4), channel_id=1, source_target_pairs={{0,1},{1,2},{2,3},{3,4},{4,5},{5,6},{6,7},{7,0},{8,9},{9,10},{10,1... | collective-permute-start | bytes 786440 | tf_op jit(solution)/shard_map/ppermute | solution.py:49
  59.0 8.0 %collective-permute-start.6 = (bf16[512,256]{1,0:T(8,128)(2,1)}, bf16[512,256]{1,0:T(8,128)(2,1)}, u32[]{:S(2)}, u32[]{:S(2)}) collective-permute-start(bf16[512,256]{1,0:T(8,128)(2,1)} %collective-permute-done.5), channel_id=1, source_target_pairs={{0,1},{1,2},{2,3},{3,4},{4,5},{5,6},{6,7},{7,0},{8,9},{9,10},{10,1... | collective-permute-start | bytes 786440 | tf_op jit(solution)/shard_map/ppermute | solution.py:49
  75.0 3.1 %copy-start.4 = (f32[2048]{0:T(1024)S(1)}, f32[2048]{0:T(1024)}, u32[]{:S(2)}) copy-start(f32[2048]{0:T(1024)} %param.15) | copy-start | bytes 24580
  75.0 3.1 %copy-start.5 = (f32[2048]{0:T(1024)S(1)}, f32[2048]{0:T(1024)}, u32[]{:S(2)}) copy-start(f32[2048]{0:T(1024)} %param.14) | copy-start | bytes 24580
  93.2 35.7 %all-to-all-start = ((bf16[4,8,24,2048]{3,2,1,0:T(8,128)(2,1)}), bf16[4,8,24,2048]{3,2,1,0:T(8,128)(2,1)}, u32[]{:S(2)}, u32[]{:S(2)}) async-start(bf16[4,8,24,2048]{3,2,1,0:T(8,128)(2,1)} %broadcast_select_fusion), calls=%async_computation | async-start | bytes 6291456 | tf_op jit(solution)/shard_map/all_to_all | solution.py:91
  142.6 4.8 %copy-start.3 = (f32[512,6]{0,1:T(8,128)S(1)}, f32[512,6]{0,1:T(8,128)}, u32[]{:S(2)}) copy-start(f32[512,6]{0,1:T(8,128)} %param.17) | copy-start | bytes 36868
  142.6 40.5 %all-to-all-start.1 = ((bf16[4,8,24,2048]{3,2,1,0:T(8,128)(2,1)}), bf16[4,8,24,2048]{3,2,1,0:T(8,128)(2,1)}, u32[]{:S(2)}, u32[]{:S(2)}) async-start(bf16[4,8,24,2048]{3,2,1,0:T(8,128)(2,1)} %bitcast.78), calls=%async_computation.1 | async-start | bytes 6291456 | tf_op jit(solution)/shard_map/all_to_all | solution.py:93
  147.4 143.5 %reduce-scatter.2.cloned.1.call-start = ((), (), s32[]{:S(2)}) async-start(), calls=%async_computation.4 | async-start | bytes 4718592 | tf_op jit(solution)/shard_map/reduce_scatter | solution.py:98
  237.9 0.9 copy-start.2
  237.9 3.3 %copy-start.6 = (bf16[64,2048]{1,0:T(8,128)(2,1)S(1)}, bf16[64,2048]{1,0:T(8,128)(2,1)}, u32[]{:S(2)}) copy-start(bf16[64,2048]{1,0:T(8,128)(2,1)} %param.22) | copy-start | bytes 786436
Sparse Core Ops, SparseCore 0:
  238.1 52.8 reduce-scatter.1
